TPU v7x, 32 devices: a whole 2x2x4 slice. The times are simulated.
32 devices in a mesh: fs: 4 (over y, x), tp: 8 (over z, core).
Axes of the slice: x: 2, y: 2, z: 4, core: 2. Of those that a mesh axis runs over, the one named last changes fastest.
Arguments:
- tokens: bfloat16 [4096, 2048], P(('fs', 'tp')), may hold values from -6 to 6
- gate_weight: bfloat16 [2048, 5632], P('fs', 'tp'), may hold values from -0.125 to 0.125
- up_weight: bfloat16 [2048, 5632], P('fs', 'tp'), may hold values from -0.125 to 0.125
- down_weight: bfloat16 [5632, 2048], P('tp', 'fs'), may hold values from -0.078125 to 0.078125
- grad_out: bfloat16 [4096, 2048], P(('fs', 'tp')), may hold values from -6 to 6
Outputs:
- grad_input: bfloat16 [4096, 2048], P(('fs', 'tp'))
- grad_gate: float32 [2048, 5632], P('fs', 'tp')
- grad_up: float32 [2048, 5632], P('fs', 'tp')
- grad_down: float32 [5632, 2048], P('tp', 'fs')
All inputs are finite; a program needn't handle non-finite values.
Results may differ from a plain program's by a relative error of at most 0.0049.
Values may be sent and summed in bfloat16 or wider, within the bound.
A program may use at most 128 MiB of HBM per device.

v0:
```python
import jax
import jax.numpy as jnp
from jax import lax
from jax.sharding import PartitionSpec as P


def over_rows(left, right):
    return lax.dot_general(
        left, right, (((0,), (0,)), ((), ())), preferred_element_type=jnp.float32
    )


def over_cols(left, right):
    return lax.dot_general(
        left, right, (((1,), (1,)), ((), ())), preferred_element_type=jnp.float32
    )


def body(tokens, gate_weight, up_weight, down_weight, grad_out):
    tok_all, cot_all = (
        lax.all_gather(tokens, "tp", axis=0, tiled=True),
        lax.all_gather(grad_out, "tp", axis=0, tiled=True),
    )
    gate_full, up_full = (
        lax.all_gather(gate_weight, "fs", axis=0, tiled=True),
        lax.all_gather(up_weight, "fs", axis=0, tiled=True),
    )
    down_full = lax.all_gather(down_weight, "fs", axis=1, tiled=True)
    gate_pre = jnp.dot(tok_all, gate_full, preferred_element_type=jnp.float32)
    up_pre = jnp.dot(tok_all, up_full, preferred_element_type=jnp.float32)
    sig_gate = jax.nn.sigmoid(gate_pre)
    active = gate_pre * sig_gate
    hidden = (active * up_pre).astype(jnp.bfloat16)
    d_hidden = over_cols(cot_all, down_full)
    d_gate = (d_hidden * up_pre * sig_gate * (1.0 + gate_pre * (1.0 - sig_gate))).astype(
        jnp.bfloat16
    )
    d_up = (d_hidden * active).astype(jnp.bfloat16)
    grad_input = lax.psum_scatter(
        over_cols(d_gate, gate_full) + over_cols(d_up, up_full),
        "tp",
        scatter_dimension=0,
        tiled=True,
    ).astype(jnp.bfloat16)
    width = gate_full.shape[1]
    summed = lax.psum_scatter(
        jnp.concatenate(
            [over_rows(tok_all, d_gate), over_rows(tok_all, d_up), over_rows(cot_all, hidden)],
            axis=1,
        ),
        "fs",
        scatter_dimension=0,
        tiled=True,
    )
    grad_gate = summed[:, :width]
    grad_up = summed[:, width : 2 * width]
    grad_down = summed[:, 2 * width :].T
    return (grad_input, grad_gate, grad_up, grad_down)


def solution(mesh):
    in_specs = (
        P(("fs", "tp"), None),
        P("fs", "tp"),
        P("fs", "tp"),
        P("tp", "fs"),
        P(("fs", "tp"), None),
    )
    out_specs = (P(("fs", "tp"), None), P("fs", "tp"), P("fs", "tp"), P("tp", "fs"))
    return jax.shard_map(body, mesh=mesh, in_specs=in_specs, out_specs=out_specs, check_vma=False)
```

profile of v0, /device:TPU:0, one launch (start us, length us, event | category | flops | bytes accessed | tf_op | source)
XLA Modules:
  0.0 514.1 jit_solution(16898894607041836768)
XLA Ops:
  7.2 0.0 all-gather.12.cloned.1.call-start
  7.2 0.7 all-gather.12.cloned.1.call-update
  7.9 0.0 all-gather.10.cloned.1.call-start
  7.9 0.7 all-gather.10.cloned.1.call-update
  8.6 0.0 all-gather.14.cloned.1.call-start
  8.7 0.7 all-gather.14.cloned.1.call-update
  9.4 0.0 all-gather.8.cloned.1.call-start
  9.4 0.5 all-gather.8.cloned.1.call-update
  10.0 0.0 all-gather.6.cloned.1.call-start
  10.0 0.5 all-gather.6.cloned.1.call-update
  10.5 0.0 reduce-scatter.3.cloned.1.call-start
  10.6 43.5 %all-gather.12.cloned.1.call-done = bf16[2048,704]{0,1:T(8,128)(2,1)} async-done(((bf16[512,704]{0,1:T(8,128)(2,1)}), bf16[2048,704]{0,1:T(8,128)(2,1)}) %all-gather.12.cloned.1.call-update) | async-done | bytes 2883600 | tf_op jit(solution)/shard_map/all_gather | solution.py:26
  54.1 48.5 %all-gather.10.cloned.1.call-done = bf16[1024,2048]{1,0:T(8,128)(2,1)} async-done(((bf16[128,2048]{1,0:T(8,128)(2,1)}), bf16[1024,2048]{1,0:T(8,128)(2,1)}) %all-gather.10.cloned.1.call-update) | async-done | bytes 4194320 | tf_op jit(solution)/shard_map/all_gather | solution.py:21
  102.6 7.8 %fusion.3 = f32[1024,704]{0,1:T(8,128)} fusion(bf16[1024,2048]{1,0:T(8,128)(2,1)} %all-gather.10.cloned.1.call-done, bf16[2048,704]{0,1:T(8,128)(2,1)} %all-gather.12.cloned.1.call-done), kind=kOutput, calls=%fused_computation.12 | convolution fusion | flops 2952790016 | bytes 9961472 | tf_op jit(solution)/shard_map/dot_general | solution.py:30
  110.4 34.4 %all-gather.14.cloned.1.call-done = bf16[2048,704]{0,1:T(8,128)(2,1)} async-done(((bf16[512,704]{0,1:T(8,128)(2,1)}), bf16[2048,704]{0,1:T(8,128)(2,1)}) %all-gather.14.cloned.1.call-update) | async-done | bytes 2883600 | tf_op jit(solution)/shard_map/all_gather | solution.py:25
  144.8 7.9 %fusion.4 = f32[1024,704]{0,1:T(8,128)} fusion(bf16[1024,2048]{1,0:T(8,128)(2,1)} %all-gather.10.cloned.1.call-done, bf16[2048,704]{0,1:T(8,128)(2,1)} %all-gather.14.cloned.1.call-done), kind=kOutput, calls=%fused_computation.13 | convolution fusion | flops 2952790016 | bytes 9961472 | tf_op jit(solution)/shard_map/dot_general | solution.py:29
  152.7 35.3 %all-gather.8.cloned.1.call-done = bf16[704,2048]{1,0:T(8,128)(2,1)} async-done(((bf16[704,512]{1,0:T(8,128)(2,1)}), bf16[704,2048]{1,0:T(8,128)(2,1)}) %all-gather.8.cloned.1.call-update) | async-done | bytes 2883600 | tf_op jit(solution)/shard_map/all_gather | solution.py:28
  188.1 48.3 %all-gather.6.cloned.1.call-done = bf16[1024,2048]{1,0:T(8,128)(2,1)} async-done(((bf16[128,2048]{1,0:T(8,128)(2,1)}), bf16[1024,2048]{1,0:T(8,128)(2,1)}) %all-gather.6.cloned.1.call-update) | async-done | bytes 4194320 | tf_op jit(solution)/shard_map/all_gather | solution.py:22
  236.4 8.6 %multiply_convert_fusion.1 = (bf16[1024,704]{0,1:T(8,128)(2,1)S(1)}, bf16[1024,704]{0,1:T(8,128)(2,1)S(1)}) fusion(f32[1024,704]{0,1:T(8,128)} %fusion.4, f32[1024,704]{0,1:T(8,128)} %fusion.3, bf16[1024,2048]{1,0:T(8,128)(2,1)} %all-gather.6.cloned.1.call-done, bf16[704,2048]{1,0:T(8,128)(2,1)} %all-gather.8.cloned.1.call-done), kind=kOutput, calls=%fused_computation.6 | convolution fusion | flops 2962161664 | bytes 15728640 | tf_op jit(solution)/shard_map/dot_general | solution.py:14
  245.1 3.5 fusion.5
  248.6 6.1 %convolution_add_fusion = f32[1024,2048]{1,0:T(8,128)} fusion(f32[1024,2048]{1,0:T(8,128)S(1)} %fusion.5, bf16[1024,704]{0,1:T(8,128)(2,1)S(1)} %get-tuple-element.4, bf16[2048,704]{0,1:T(8,128)(2,1)S(1)} %copy-done.2), kind=kOutput, calls=%fused_computation.1 | convolution fusion | flops 2954887168 | bytes 21102592 | tf_op jit(solution)/shard_map/dot_general | solution.py:14
  254.8 0.0 reduce-scatter.5.cloned.1.call-start
  254.8 1.3 copy-done.5
  256.1 5.1 convolution_bitcast_fusion.1
  261.2 3.2 convolution_bitcast_fusion.2
  264.4 0.7 copy-done.9
  265.1 3.2 convolution_bitcast_fusion
  268.3 6.5 %pad_maximum_fusion = f32[2048,2112]{0,1:T(8,128)} fusion(f32[2048,704]{0,1:T(8,128)S(1)} %convolution_bitcast_fusion, f32[2048,704]{0,1:T(8,128)S(1)} %convolution_bitcast_fusion.1, f32[2048,704]{0,1:T(8,128)S(1)} %convolution_bitcast_fusion.2), kind=kLoop, calls=%fused_computation | loop fusion | flops 8650752 | bytes 34603008 | tf_op jit(solution)/shard_map/concatenate | solution.py:47
  274.9 68.4 %reduce-scatter.3.cloned.1.call-done = f32[128,2048]{1,0:T(8,128)} async-done(((f32[1024,2048]{1,0:T(8,128)}), f32[128,2048]{1,0:T(8,128)}) %reduce-scatter.3.cloned.1.call-update) | async-done | bytes 1048592 | tf_op jit(solution)/shard_map/reduce_scatter | solution.py:39
  343.2 2.1 convert_element_type.14
  345.3 157.5 %reduce-scatter.5.cloned.1.call-done = f32[512,2112]{0,1:T(8,128)} async-done(((f32[2048,2112]{0,1:T(8,128)}), f32[512,2112]{0,1:T(8,128)}) %reduce-scatter.5.cloned.1.call-update) | async-done | bytes 4325392 | tf_op jit(solution)/shard_map/reduce_scatter | solution.py:46
  502.8 4.4 slice_bitcast_fusion
  (20 shorter events, 0.1 us)
Async XLA Ops:
  7.2 46.9 %all-gather.12.cloned.1.call-start = ((), (), s32[]{:S(2)}) async-start(), calls=%async_computation.5 | async-start | bytes 3604480 | tf_op jit(solution)/shard_map/all_gather | solution.py:26
  7.9 94.7 %all-gather.10.cloned.1.call-start = ((), (), s32[]{:S(2)}) async-start(), calls=%async_computation.4 | async-start | bytes 4718592 | tf_op jit(solution)/shard_map/all_gather | solution.py:21
  8.6 136.2 %all-gather.14.cloned.1.call-start = ((), (), s32[]{:S(2)}) async-start(), calls=%async_computation.6 | async-start | bytes 3604480 | tf_op jit(solution)/shard_map/all_gather | solution.py:25
  9.4 178.7 %all-gather.8.cloned.1.call-start = ((), (), s32[]{:S(2)}) async-start(), calls=%async_computation.3 | async-start | bytes 3604480 | tf_op jit(solution)/shard_map/all_gather | solution.py:28
  10.0 226.4 %all-gather.6.cloned.1.call-start = ((), (), s32[]{:S(2)}) async-start(), calls=%async_computation.2 | async-start | bytes 4718592 | tf_op jit(solution)/shard_map/all_gather | solution.py:22
  10.5 332.7 %reduce-scatter.3.cloned.1.call-start = ((), (), s32[]{:S(2)}) async-start(), calls=%async_computation.7 | async-start | bytes 9437184 | tf_op jit(solution)/shard_map/reduce_scatter | solution.py:39
  152.7 92.3 %copy-start.3 = (bf16[2048,704]{0,1:T(8,128)(2,1)S(1)}, bf16[2048,704]{0,1:T(8,128)(2,1)}, u32[]{:S(2)}) copy-start(bf16[2048,704]{0,1:T(8,128)(2,1)} %all-gather.14.cloned.1.call-done) | copy-start | bytes 8650756
  245.0 3.6 copy-start.6
  245.0 3.6 copy-start.4
  245.1 3.6 copy-start.2
  254.7 1.4 copy-start.5
  254.7 6.4 %copy-start.7 = (bf16[1024,704]{0,1:T(8,128)(2,1)S(1)}, bf16[1024,704]{0,1:T(8,128)(2,1)}, u32[]{:S(2)}) copy-start(bf16[1024,704]{0,1:T(8,128)(2,1)} %copy-done.6) | copy-start | bytes 4325380
  254.8 248.1 %reduce-scatter.5.cloned.1.call-start = ((), (), s32[]{:S(2)}) async-start(), calls=%async_computation.8 | async-start | bytes 21626880 | tf_op jit(solution)/shard_map/reduce_scatter | solution.py:46
  256.1 5.1 copy-start
  261.2 3.2 copy-start.1
  261.2 3.2 copy-start.8
  261.2 3.9 copy-start.9
Sparse Core Ops, SparseCore 0:
  9.8 44.2 all-gather.11
  55.7 46.8 all-gather.9
  104.4 40.3 all-gather.13
  146.5 41.5 all-gather.7
  189.5 46.8 all-gather.5
  254.9 88.3 reduce-scatter.2
  346.4 156.4 reduce-scatter.4
where the time goes:
time: 514 us
  waiting for transfers between devices  439 us (85%)
  matrix products  45.4 us (9%)
  between operations  14.3 us (3%)
  other arithmetic  8.6 us (2%)
  local copies, waits for them, and re-layouts  6.37 us (1%)
    reduce_scatter x1, waiting for transfers between devices, body(): lax.psum_scatter(jnp.concatenate([over_rows(tok_all, d_gate), over_rows(t...  158 us
    reduce_scatter x1, waiting for transfers between devices, body(): lax.psum_scatter(over_cols(d_gate, gate_full) + over_cols(d_up, up_full),...  68.4 us
    all_gather x1, waiting for transfers between devices, body(): lax.all_gather(tokens, 'tp', axis=0, tiled=True)  48.5 us
    all_gather x1, waiting for transfers between devices, body(): lax.all_gather(grad_out, 'tp', axis=0, tiled=True)  48.3 us
    all_gather x1, waiting for transfers between devices, body(): lax.all_gather(up_weight, 'fs', axis=0, tiled=True)  43.5 us
    all_gather x1, waiting for transfers between devices, body(): down_full = lax.all_gather(down_weight, 'fs', axis=1, tiled=True)  35.3 us
    all_gather x1, waiting for transfers between devices, body(): lax.all_gather(gate_weight, 'fs', axis=0, tiled=True)  34.4 us
    dot_general x3, matrix products, over_cols(): lax.dot_general(left, right, (((1,), (1,)), ((), ())), preferred_element_...  18.2 us
  transfers between devices with their start and end apart: 7, of which 7 were waited for; matrix products, arithmetic and copies ran while one was open for 7% of the time, Pallas kernels for 0%

commit v1 on v0

--- a/solution.py
+++ b/solution.py
@@ -25,7 +25,13 @@
         lax.all_gather(gate_weight, "fs", axis=0, tiled=True),
         lax.all_gather(up_weight, "fs", axis=0, tiled=True),
     )
-    down_full = lax.all_gather(down_weight, "fs", axis=1, tiled=True)
+    size = lax.axis_size("fs")
+    moving, blocks = (down_weight, [down_weight])
+    for _ in range(size - 1):
+        moving = lax.ppermute(moving, "fs", [(i, (i + 1) % size) for i in range(size)])
+        blocks.insert(0, moving)
+    merged = jnp.concatenate(blocks, axis=1)
+    down_full = jnp.roll(merged, (lax.axis_index("fs") + 1) * down_weight.shape[1], axis=1)
     gate_pre = jnp.dot(tok_all, gate_full, preferred_element_type=jnp.float32)
     up_pre = jnp.dot(tok_all, up_full, preferred_element_type=jnp.float32)
     sig_gate = jax.nn.sigmoid(gate_pre)

time: 514 us -> 491 us (0.955)
  waiting for transfers between devices: 439 us -> 402 us
  local copies, waits for them, and re-layouts: 6.37 us -> 14.4 us
  starting transfers between devices: 0.27 us -> 6.22 us
    ppermute x0 -> x3, waiting for transfers between devices: none -> 69.2 us  [body(): lax.ppermute(moving, 'fs', [(i, (i + 1) % size) for i in range(size)])]
    all_gather x1 -> x0, waiting for transfers between devices: 35.3 us -> none  [body(): down_full = lax.all_gather(down_weight, 'fs', axis=1, tiled=True)]
    all_gather x1, waiting for transfers between devices: 34.4 us -> 0.01 us  [body(): lax.all_gather(gate_weight, 'fs', axis=0, tiled=True)]
    all_gather x1, waiting for transfers between devices: 48.5 us -> 29.6 us  [body(): lax.all_gather(tokens, 'tp', axis=0, tiled=True)]
    all_gather x1, waiting for transfers between devices: 43.5 us -> 34.4 us  [body(): lax.all_gather(up_weight, 'fs', axis=0, tiled=True)]
    all_gather x1, waiting for transfers between devices: 48.3 us -> 40.5 us  [body(): lax.all_gather(grad_out, 'tp', axis=0, tiled=True)]
    unnamed x20 -> x29, local copies, waits for them, and re-layouts: 1.99 us -> 8.97 us
    ppermute x0 -> x3, starting transfers between devices: none -> 5.99 us  [body(): lax.ppermute(moving, 'fs', [(i, (i + 1) % size) for i in range(size)])]
  transfers between devices with their start and end apart: 7 -> 9, of which waited for: 7 -> 8; matrix products, arithmetic and copies ran while one was open for 7% -> 9% of each run, Pallas kernels for 0% -> 0%
where the time goes in v1:
time: 491 us
  waiting for transfers between devices  402 us (82%)
  matrix products  45.5 us (9%)
  local copies, waits for them, and re-layouts  14.4 us (3%)
  between operations  14.3 us (3%)
  other arithmetic  8.63 us (2%)
  starting transfers between devices  6.22 us (1%)
    reduce_scatter x1, waiting for transfers between devices, body(): lax.psum_scatter(jnp.concatenate([over_rows(tok_all, d_gate), over_rows(t...  157 us
    ppermute x3, waiting for transfers between devices, body(): lax.ppermute(moving, 'fs', [(i, (i + 1) % size) for i in range(size)])  69.2 us
    reduce_scatter x1, waiting for transfers between devices, body(): lax.psum_scatter(over_cols(d_gate, gate_full) + over_cols(d_up, up_full),...  68.3 us
    all_gather x1, waiting for transfers between devices, body(): lax.all_gather(grad_out, 'tp', axis=0, tiled=True)  40.5 us
    all_gather x1, waiting for transfers between devices, body(): lax.all_gather(up_weight, 'fs', axis=0, tiled=True)  34.4 us
    all_gather x1, waiting for transfers between devices, body(): lax.all_gather(tokens, 'tp', axis=0, tiled=True)  29.6 us
    dot_general x3, matrix products, over_cols(): lax.dot_general(left, right, (((1,), (1,)), ((), ())), preferred_element_...  18.3 us
    dot_general x3, matrix products, over_rows(): lax.dot_general(left, right, (((0,), (0,)), ((), ())), preferred_element_...  11.5 us
  transfers between devices with their start and end apart: 9, of which 8 were waited for; matrix products, arithmetic and copies ran while one was open for 9% of the time, Pallas kernels for 0%

profile of v1, /device:TPU:0, one launch (start us, length us, event | category | flops | bytes accessed | tf_op | source)
XLA Modules:
  0.0 490.9 jit_solution(16946775046541042557)
XLA Ops:
  7.9 0.7 all-gather.7.cloned.1.call-update
  10.0 3.0 collective-permute-start
  13.0 24.7 %collective-permute-done = bf16[704,512]{1,0:T(8,128)(2,1)S(1)} collective-permute-done((bf16[704,512]{1,0:T(8,128)(2,1)}, bf16[704,512]{1,0:T(8,128)(2,1)S(1)}, u32[]{:S(2)}, u32[]{:S(2)}) %collective-permute-start) | collective-permute-done | bytes 720928 | tf_op jit(solution)/shard_map/ppermute | solution.py:31
  37.8 1.1 collective-permute-start.1
  38.8 28.5 %collective-permute-done.1 = bf16[704,512]{1,0:T(8,128)(2,1)S(1)} collective-permute-done((bf16[704,512]{1,0:T(8,128)(2,1)S(1)}, bf16[704,512]{1,0:T(8,128)(2,1)S(1)}, u32[]{:S(2)}, u32[]{:S(2)}) %collective-permute-start.1) | collective-permute-done | bytes 720928 | tf_op jit(solution)/shard_map/ppermute | solution.py:31
  67.4 1.9 collective-permute-start.2
  69.3 15.9 %collective-permute-done.2 = bf16[704,512]{1,0:T(8,128)(2,1)S(1)} collective-permute-done((bf16[704,512]{1,0:T(8,128)(2,1)S(1)}, bf16[704,512]{1,0:T(8,128)(2,1)S(1)}, u32[]{:S(2)}, u32[]{:S(2)}) %collective-permute-start.2) | collective-permute-done | bytes 720928 | tf_op jit(solution)/shard_map/ppermute | solution.py:31
  85.2 1.0 constant_dynamic-update-slice_fusion.7
  86.2 1.1 constant_dynamic-update-slice_fusion.6
  87.3 0.9 constant_dynamic-update-slice_fusion.5
  88.2 1.0 constant_dynamic-update-slice_fusion.4
  89.2 1.0 constant_dynamic-update-slice_fusion.3
  90.2 1.0 constant_dynamic-update-slice_fusion.2
  91.2 1.0 constant_dynamic-update-slice_fusion.1
  92.1 1.0 constant_dynamic-update-slice_fusion
  93.2 29.6 %all-gather.7.cloned.1.call-done = bf16[1024,2048]{1,0:T(8,128)(2,1)} async-done(((bf16[128,2048]{1,0:T(8,128)(2,1)}), bf16[1024,2048]{1,0:T(8,128)(2,1)}) %all-gather.7.cloned.1.call-update) | async-done | bytes 4194320 | tf_op jit(solution)/shard_map/all_gather | solution.py:21
  122.7 7.8 %fusion.11 = f32[1024,704]{0,1:T(8,128)} fusion(bf16[1024,2048]{1,0:T(8,128)(2,1)} %all-gather.7.cloned.1.call-done, bf16[2048,704]{0,1:T(8,128)(2,1)} %all-gather.11.cloned.1.call-done), kind=kOutput, calls=%fused_computation.28 | convolution fusion | flops 2952790016 | bytes 9961472 | tf_op jit(solution)/shard_map/dot_general | solution.py:35
  130.5 34.4 %all-gather.9.cloned.1.call-done = bf16[2048,704]{0,1:T(8,128)(2,1)} async-done(((bf16[512,704]{0,1:T(8,128)(2,1)}), bf16[2048,704]{0,1:T(8,128)(2,1)}) %all-gather.9.cloned.1.call-update) | async-done | bytes 2883600 | tf_op jit(solution)/shard_map/all_gather | solution.py:26
  164.9 7.9 %fusion.10 = f32[1024,704]{0,1:T(8,128)} fusion(bf16[1024,2048]{1,0:T(8,128)(2,1)} %all-gather.7.cloned.1.call-done, bf16[2048,704]{0,1:T(8,128)(2,1)} %all-gather.9.cloned.1.call-done), kind=kOutput, calls=%fused_computation.27 | convolution fusion | flops 2952790016 | bytes 9961472 | tf_op jit(solution)/shard_map/dot_general | solution.py:36
  172.8 40.5 %all-gather.5.cloned.1.call-done = bf16[1024,2048]{1,0:T(8,128)(2,1)} async-done(((bf16[128,2048]{1,0:T(8,128)(2,1)}), bf16[1024,2048]{1,0:T(8,128)(2,1)}) %all-gather.5.cloned.1.call-update) | async-done | bytes 4194320 | tf_op jit(solution)/shard_map/all_gather | solution.py:22
  213.3 8.7 %fusion.3 = (bf16[1024,704]{0,1:T(8,128)(2,1)S(1)}, bf16[1024,704]{0,1:T(8,128)(2,1)S(1)}) fusion(f32[1024,704]{0,1:T(8,128)} %fusion.11, f32[1024,704]{0,1:T(8,128)} %fusion.10, bf16[1024,2048]{1,0:T(8,128)(2,1)} %all-gather.5.cloned.1.call-done, bf16[704,4096]{1,0:T(8,128)(2,1)} %constant_dynamic-update-slice_fusion, s32[]{:T(128)S(6)} %select_n.14), kind=kOutput, calls=%fused_computation.10 | convolution fusion | flops 2962161664 | bytes 15728644 | tf_op jit(solution)/shard_map/dot_general | solution.py:14
  222.0 3.7 fusion.12
  225.7 6.0 %convolution_add_fusion = f32[1024,2048]{1,0:T(8,128)} fusion(f32[1024,2048]{1,0:T(8,128)S(1)} %fusion.12, bf16[1024,704]{0,1:T(8,128)(2,1)S(1)} %get-tuple-element.4, bf16[2048,704]{0,1:T(8,128)(2,1)S(1)} %copy-done.4), kind=kOutput, calls=%fused_computation.1 | convolution fusion | flops 2954887168 | bytes 21102592 | tf_op jit(solution)/shard_map/dot_general | solution.py:14
  231.8 1.3 copy-done.6
  233.1 5.1 %convolution_bitcast_fusion.1 = f32[2048,704]{0,1:T(8,128)S(1)} fusion(bf16[1024,704]{0,1:T(8,128)(2,1)S(1)} %copy-done.6, bf16[1024,2048]{1,0:T(8,128)(2,1)} %all-gather.7.cloned.1.call-done), kind=kOutput, calls=%fused_computation.3 | convolution fusion | flops 2952790016 | bytes 11403264 | tf_op jit(solution)/shard_map/dot_general | solution.py:8
  238.2 3.2 convolution_bitcast_fusion.2
  242.1 3.2 convolution_bitcast_fusion
  245.3 6.5 %pad_maximum_fusion = f32[2048,2112]{0,1:T(8,128)} fusion(f32[2048,704]{0,1:T(8,128)S(1)} %convolution_bitcast_fusion, f32[2048,704]{0,1:T(8,128)S(1)} %convolution_bitcast_fusion.1, f32[2048,704]{0,1:T(8,128)S(1)} %convolution_bitcast_fusion.2), kind=kLoop, calls=%fused_computation | loop fusion | flops 8650752 | bytes 34603008 | tf_op jit(solution)/shard_map/concatenate | solution.py:53
  251.9 68.3 %reduce-scatter.3.cloned.1.call-done = f32[128,2048]{1,0:T(8,128)} async-done(((f32[1024,2048]{1,0:T(8,128)}), f32[128,2048]{1,0:T(8,128)}) %reduce-scatter.3.cloned.1.call-update) | async-done | bytes 1048592 | tf_op jit(solution)/shard_map/reduce_scatter | solution.py:45
  320.2 2.1 convert_element_type.14
  322.3 157.4 %reduce-scatter.5.cloned.1.call-done = f32[512,2112]{0,1:T(8,128)} async-done(((f32[2048,2112]{0,1:T(8,128)}), f32[512,2112]{0,1:T(8,128)}) %reduce-scatter.5.cloned.1.call-update) | async-done | bytes 4325392 | tf_op jit(solution)/shard_map/reduce_scatter | solution.py:52
  479.7 4.4 slice_bitcast_fusion
  (33 shorter events, 2.9 us)
Async XLA Ops:
  7.2 86.0 %all-gather.11.cloned.1.call-start = ((), (), s32[]{:S(2)}) async-start(), calls=%async_computation.5 | async-start | bytes 3604480 | tf_op jit(solution)/shard_map/all_gather | solution.py:25
  7.9 114.8 %all-gather.7.cloned.1.call-start = ((), (), s32[]{:S(2)}) async-start(), calls=%async_computation.3 | async-start | bytes 4718592 | tf_op jit(solution)/shard_map/all_gather | solution.py:21
  8.6 79.6 %copy-start = (bf16[704,512]{1,0:T(8,128)(2,1)S(1)}, bf16[704,512]{1,0:T(8,128)(2,1)}, u32[]{:S(2)}) copy-start(bf16[704,512]{1,0:T(8,128)(2,1)} %param.8) | copy-start | bytes 2162692
  8.7 156.3 %all-gather.9.cloned.1.call-start = ((), (), s32[]{:S(2)}) async-start(), calls=%async_computation.4 | async-start | bytes 3604480 | tf_op jit(solution)/shard_map/all_gather | solution.py:26
  9.4 203.9 %all-gather.5.cloned.1.call-start = ((), (), s32[]{:S(2)}) async-start(), calls=%async_computation.2 | async-start | bytes 4718592 | tf_op jit(solution)/shard_map/all_gather | solution.py:22
  10.0 310.3 %reduce-scatter.3.cloned.1.call-start = ((), (), s32[]{:S(2)}) async-start(), calls=%async_computation.6 | async-start | bytes 9437184 | tf_op jit(solution)/shard_map/reduce_scatter | solution.py:45
  10.0 27.8 %collective-permute-start = (bf16[704,512]{1,0:T(8,128)(2,1)}, bf16[704,512]{1,0:T(8,128)(2,1)S(1)}, u32[]{:S(2)}, u32[]{:S(2)}) collective-permute-start(bf16[704,512]{1,0:T(8,128)(2,1)} %param.8), channel_id=1, source_target_pairs={{0,8},{8,16},{16,24},{24,0},{1,9},{9,17},{17,25},{25,1},{2,10},{10... | collective-permute-start | bytes 2162696 | tf_op jit(solution)/shard_map/ppermute | solution.py:31
  37.8 29.6 %collective-permute-start.1 = (bf16[704,512]{1,0:T(8,128)(2,1)S(1)}, bf16[704,512]{1,0:T(8,128)(2,1)S(1)}, u32[]{:S(2)}, u32[]{:S(2)}) collective-permute-start(bf16[704,512]{1,0:T(8,128)(2,1)S(1)} %collective-permute-done), channel_id=1, source_target_pairs={{0,8},{8,16},{16,24},{24,0},{1,9},{9,17},{17,25},{25,1},{2,10},{10... | collective-permute-start | bytes 2162696 | tf_op jit(solution)/shard_map/ppermute | solution.py:31
  67.4 17.8 %collective-permute-start.2 = (bf16[704,512]{1,0:T(8,128)(2,1)S(1)}, bf16[704,512]{1,0:T(8,128)(2,1)S(1)}, u32[]{:S(2)}, u32[]{:S(2)}) collective-permute-start(bf16[704,512]{1,0:T(8,128)(2,1)S(1)} %collective-permute-done.1), channel_id=1, source_target_pairs={{0,8},{8,16},{16,24},{24,0},{1,9},{9,17},{17,25},{25,1},{2,10},{10... | collective-permute-start | bytes 2162696 | tf_op jit(solution)/shard_map/ppermute | solution.py:31
  172.8 49.2 %copy-start.3 = (bf16[2048,704]{0,1:T(8,128)(2,1)S(1)}, bf16[2048,704]{0,1:T(8,128)(2,1)}, u32[]{:S(2)}) copy-start(bf16[2048,704]{0,1:T(8,128)(2,1)} %all-gather.11.cloned.1.call-done) | copy-start | bytes 8650756
  222.0 3.8 copy-start.7
  222.0 3.8 copy-start.5
  222.0 3.7 copy-start.4
  231.7 1.4 copy-start.6
  231.7 6.4 %copy-start.8 = (bf16[1024,704]{0,1:T(8,128)(2,1)S(1)}, bf16[1024,704]{0,1:T(8,128)(2,1)}, u32[]{:S(2)}) copy-start(bf16[1024,704]{0,1:T(8,128)(2,1)} %copy-done.7) | copy-start | bytes 4325380
  231.8 247.9 %reduce-scatter.5.cloned.1.call-start = ((), (), s32[]{:S(2)}) async-start(), calls=%async_computation.7 | async-start | bytes 21626880 | tf_op jit(solution)/shard_map/reduce_scatter | solution.py:52
  233.1 5.1 %copy-start.1 = (bf16[1024,2048]{1,0:T(8,128)(2,1)S(1)}, bf16[1024,2048]{1,0:T(8,128)(2,1)}, u32[]{:S(2)}) copy-start(bf16[1024,2048]{1,0:T(8,128)(2,1)} %all-gather.7.cloned.1.call-done) | copy-start | bytes 12582916
  238.2 3.2 copy-start.2
  238.2 3.2 copy-start.9
  238.2 3.9 copy-start.10
Sparse Core Ops, SparseCore 0:
  9.8 64.7 all-gather.10
  76.1 46.5 all-gather.6
  124.6 40.3 all-gather.8
  166.4 46.8 all-gather.4
  231.9 88.3 reduce-scatter.2
  323.2 156.4 reduce-scatter.4
